TPU v7x, 1024 devices: a 2x16x16 block of a 4x16x16 slice. The times are simulated.
1024 devices in a mesh: grp: 2 (over x), fs: 16 (over z), tp: 32 (over y, core).
Axes of the slice: x: 2, y: 16, z: 16, core: 2. Of those that a mesh axis runs over, the one named last changes fastest.
The devices are a block of a 4x16x16 slice.
Arguments:
- tokens: bfloat16 [4096, 3584], P(('grp', 'fs')), parts along dimension 0, may hold values from -6 to 6
- norm_gain: float32 [3584], P('fs'), may hold values from 0.1 to 1.9
- up_master: float32 [3584, 14336], P('fs', 'tp'), may hold values from -0.09375 to 0.09375
- down_master: float32 [3584, 14336], P('fs', 'tp'), may hold values from -0.046875 to 0.046875
Outputs:
- up_ready: bfloat16 [7168, 14336], P('grp', 'tp'), parts along dimension 0
- down_ready: bfloat16 [7168, 14336], P('grp', 'tp'), parts along dimension 0
- mixed_out: bfloat16 [4096, 3584], P(('grp', 'fs', 'tp')), parts along dimension 0
There are 2 independent parts, one for each index of `grp`. A program takes and returns all parts, laid end to end along the dimension named above; an argument that names none is the same for every part. Nothing has to cross between parts.
All inputs are finite; a program needn't handle non-finite values.
Results may differ from a plain program's by a relative error of at most 0.024.
Values may be sent and summed in bfloat16 or wider, within the bound.
A program may use at most 64 MiB of HBM per device.

v0:
```python
import jax
import jax.numpy as jnp
from jax import lax
from jax.sharding import PartitionSpec as P


def sent_together(arrays, axis, dim, along):
    widths = [a.shape[along] for a in arrays]
    both = jnp.concatenate(arrays, axis=along)
    result = lax.all_gather(both, axis, axis=dim, tiled=True)
    return tuple(jnp.split(result, [sum(widths[:k]) for k in range(1, len(widths))], axis=along))


def cut_along(array, dim, size):
    before, after = (array.shape[:dim], array.shape[dim + 1 :])
    return jnp.moveaxis(array.reshape(*before, size, -1, *after), dim, 0)


def summed_on_arrival(array, axis, dim):
    size = lax.axis_size(axis)
    parts = lax.all_to_all(cut_along(array, dim, size), axis, 0, 0, tiled=True)
    return jnp.sum(parts.astype(jnp.float32), axis=0)


def per_device(tokens, norm_gain, up_master, down_master):
    up_local = (norm_gain[:, None] * up_master).astype(jnp.bfloat16)
    down_local = down_master.astype(jnp.bfloat16)
    values = tokens.astype(jnp.float32)
    square_mean = jnp.mean(values * values, axis=1, keepdims=True)
    normed = (values * lax.rsqrt(square_mean + 1e-06)).astype(jnp.bfloat16)
    up_ready, down_ready = sent_together((up_local, down_local), "fs", 0, 1)
    up_acts = jnp.dot(normed, up_ready, preferred_element_type=jnp.float32)
    hidden = jnp.square(jax.nn.relu(up_acts)).astype(jnp.bfloat16)
    mixed_out = summed_on_arrival(
        lax.dot_general(
            hidden, down_ready, (((1,), (1,)), ((), ())), preferred_element_type=jnp.float32
        ).astype(jnp.bfloat16),
        "tp",
        0,
    ).astype(jnp.bfloat16)
    return (up_ready, down_ready, mixed_out)


def solution(mesh):
    return jax.shard_map(
        per_device,
        mesh=mesh,
        in_specs=(P(("grp", "fs"), None), P("fs"), P("fs", "tp"), P("fs", "tp")),
        out_specs=(P("grp", "tp"), P("grp", "tp"), P(("grp", "fs", "tp"), None)),
        check_vma=False,
    )
```

profile of v0, /device:TPU:5, one launch (start us, length us, event | category | flops | bytes accessed | tf_op | source)
XLA Modules:
  0.0 258.0 jit_solution(8517597311001194873)
XLA Ops:
  7.2 0.1 all-gather.2.cloned.1.call-start
  7.2 1.0 convert_element_type.21
  8.3 1.1 multiply_convert_fusion
  9.4 0.9 pad_maximum_fusion
  10.3 0.1 all-gather.2.cloned.1.call-update
  10.4 1.4 fusion
  11.8 168.8 %all-gather.2.cloned.1.call-done = bf16[3584,896]{1,0:T(8,128)(2,1)} async-done(((bf16[224,896]{1,0:T(8,128)(2,1)}), bf16[3584,896]{1,0:T(8,128)(2,1)}) %all-gather.2.cloned.1.call-update) | async-done | bytes 6422544 | tf_op jit(solution)/shard_map/all_gather | solution.py:10
  180.6 5.5 %convolution_convert_fusion = bf16[128,3584]{1,0:T(8,128)(2,1)S(1)} fusion(bf16[128,3584]{1,0:T(8,128)(2,1)} %param.4, f32[128]{0:T(128)S(1)} %add_rsqrt_fusion, bf16[3584,896]{1,0:T(8,128)(2,1)} %all-gather.2.cloned.1.call-done), kind=kOutput, calls=%fused_computation | convolution fusion | flops 824090624 | bytes 9175552 | tf_op jit(solution)/shard_map/dot_general | solution.py:35
  186.1 1.1 reshape.18
  187.2 13.0 %all-to-all-start = ((bf16[32,4,3584]{2,1,0:T(4,128)(2,1)}), bf16[32,4,3584]{2,1,0:T(4,128)(2,1)S(1)}, u32[]{:S(2)}, u32[]{:S(2)}) async-start(bf16[32,4,3584]{2,1,0:T(4,128)(2,1)} %reshape.18), calls=%async_computation | async-start | bytes 1835008 | tf_op jit(solution)/shard_map/all_to_all | solution.py:21
  200.3 8.4 %fusion.13 = (bf16[3584,448]{1,0:T(8,128)(2,1)}, bf16[3584,448]{1,0:T(8,128)(2,1)}) fusion(bf16[3584,896]{1,0:T(8,128)(2,1)} %all-gather.2.cloned.1.call-done), kind=kLoop, calls=%fused_computation.16 | loop fusion | bytes 12845056 | tf_op jit(solution)/shard_map/split | solution.py:11
  208.6 5.7 %copy.10 = bf16[3584,448]{0,1:T(8,128)(2,1)} copy(bf16[3584,448]{1,0:T(8,128)(2,1)} %get-tuple-element.6) | data formatting | bytes 6422528
  214.3 5.7 %copy.9 = bf16[3584,448]{0,1:T(8,128)(2,1)} copy(bf16[3584,448]{1,0:T(8,128)(2,1)} %get-tuple-element.7) | data formatting | bytes 6422528
  220.0 30.2 %all-to-all-done = bf16[32,4,3584]{2,1,0:T(4,128)(2,1)S(1)} async-done(((bf16[32,4,3584]{2,1,0:T(4,128)(2,1)}), bf16[32,4,3584]{2,1,0:T(4,128)(2,1)S(1)}, u32[]{:S(2)}, u32[]{:S(2)}) %all-to-all-start) | async-done | bytes 917536 | tf_op jit(solution)/shard_map/all_to_all | solution.py:21
  250.2 1.0 reduce_sum.22
  (1 shorter events, 0.0 us)
Async XLA Ops:
  7.2 173.5 %all-gather.2.cloned.1.call-start = ((), (), s32[]{:S(2)}) async-start(), calls=%async_computation.1 | async-start | bytes 6823936 | tf_op jit(solution)/shard_map/all_gather | solution.py:10
  187.2 62.9 %all-to-all-start = ((bf16[32,4,3584]{2,1,0:T(4,128)(2,1)}), bf16[32,4,3584]{2,1,0:T(4,128)(2,1)S(1)}, u32[]{:S(2)}, u32[]{:S(2)}) async-start(bf16[32,4,3584]{2,1,0:T(4,128)(2,1)} %reshape.18), calls=%async_computation | async-start | bytes 1835008 | tf_op jit(solution)/shard_map/all_to_all | solution.py:21
Sparse Core Ops, SparseCore 0:
  11.3 169.3 all-gather.1
where the time goes:
time: 259 us; the launch traced here: 258 us
  waiting for transfers between devices  199 us (77%)
  local copies, waits for them, and re-layouts  20.8 us (8%)
  between operations  14.1 us (5%)
  starting transfers between devices  13.1 us (5%)
  other arithmetic  5.49 us (2%)
  matrix products  5.45 us (2%)
    all_gather x1, waiting for transfers between devices, sent_together(): result = lax.all_gather(both, axis, axis=dim, tiled=True)  169 us
    all_to_all x1, waiting for transfers between devices, summed_on_arrival(): parts = lax.all_to_all(cut_along(array, dim, size), axis, 0, 0, tiled=True)  30.2 us
    all_to_all x1, starting transfers between devices, summed_on_arrival(): parts = lax.all_to_all(cut_along(array, dim, size), axis, 0, 0, tiled=True)  13 us
    unnamed x2, local copies, waits for them, and re-layouts  11.3 us
    split x1, local copies, waits for them, and re-layouts, sent_together(): jnp.split(result, [sum(widths[:k]) for k in range(1, len(widths))], axis=...  8.35 us
    dot_general x1, matrix products, per_device(): lax.dot_general(hidden, down_ready, (((1,), (1,)), ((), ())), preferred_e...  5.45 us
  transfers between devices with their start and end apart: 2, of which 2 were waited for; matrix products, arithmetic and copies ran while one was open for 8% of the time, Pallas kernels for 0%

commit v1 on v0

v1 whole, which is shorter than its diff:
```python
import functools

import jax
import jax.numpy as jnp
from jax import lax
from jax.experimental import pallas as pl
from jax.experimental.pallas import tpu as pltpu
from jax.sharding import PartitionSpec as P

MESH = pl.DeviceIdType.MESH
LANES = 128
TILE = 16
GROUPS = 4
CORES = 2
BF16, F32 = jnp.bfloat16, jnp.float32


def pack_rows(rows, cols):
    whole = cols // LANES * LANES
    return rows * (whole // LANES) + rows * (cols - whole) // LANES


def pack(value, ref, base):
    rows, cols = value.shape
    whole = cols // LANES
    for k in range(whole):
        ref[pl.ds(base + k * rows, rows), :] = value[:, k * LANES : (k + 1) * LANES]
    if cols % LANES:
        part = rows // GROUPS
        rest = value[:, whole * LANES :]
        side = jnp.concatenate([rest[k * part : (k + 1) * part] for k in range(GROUPS)], axis=1)
        for k in range(side.shape[1] // LANES):
            ref[pl.ds(base + whole * rows + k * part, part), :] = side[:, k * LANES : (k + 1) * LANES]


def unpack(ref, base, rows, cols):
    whole = cols // LANES
    parts = [ref[pl.ds(base + k * rows, rows), :] for k in range(whole)]
    width = cols - whole * LANES
    if width:
        part = rows // GROUPS
        side = jnp.concatenate(
            [ref[pl.ds(base + whole * rows + k * part, part), :] for k in range(GROUPS * width // LANES)], axis=1
        )
        parts.append(jnp.concatenate([side[:, k * width : (k + 1) * width] for k in range(GROUPS)], axis=0))
    return jnp.concatenate(parts, axis=1)


def main_kernel(
    nz, ntp, rows, cols,
    tokens, gain, up_master, down_master,
    up_all, down_all, mixed,
    tok, gain_v, up_f, down_f, normed, acts, hid, own, pair_out, pair_in, msg_out, msg_in, keep,
    load_sem, zsend, zrecv, xsend, xrecv, psend, precv, ysend, yrecv,
):
    g, z, t = lax.axis_index("grp"), lax.axis_index("fs"), lax.axis_index("tp")
    y, c = t // CORES, t % CORES
    ny = ntp // CORES
    role = g % 2
    half_ring = nz // 2
    z_r, z_l = (z + 1) % nz, (z + nz - 1) % nz
    g_x = g + 1 - 2 * role
    t_core = t + 1 - 2 * c
    size = pack_rows(cols, rows)
    tiles = size // TILE
    e_tiles = tiles // 3
    s_tiles = tiles - 2 * e_tiles
    e_rows, s_rows = e_tiles * TILE, s_tiles * TILE
    q = mixed.shape[1]
    n_tok = tok.shape[0]
    gathers = (up_all, down_all)

    loads = [
        pltpu.make_async_copy(src, dst, load_sem.at[k])
        for k, (src, dst) in enumerate(((up_master, up_f), (gain, gain_v), (down_master, down_f), (tokens, tok)))
    ]
    for copy in loads:
        copy.start()

    def peer(k):
        return {"tp": ((y + k) % ny) * CORES + c}

    barrier = pltpu.get_barrier_semaphore()
    greeted = [{"fs": z_r}, {"fs": z_l}, {"grp": g_x}, {"tp": t_core}]
    for who in greeted:
        pl.semaphore_signal(barrier, inc=1, device_id=who, device_id_type=MESH)

    @pl.loop(1, ny)
    def _(k):
        pl.semaphore_signal(barrier, inc=1, device_id=peer(k), device_id_type=MESH)

    my_base = pl.multiple_of(z * size, TILE)
    loads[0].wait()
    loads[1].wait()
    pack((gain_v[...] * up_f[...].T).astype(BF16), up_all, my_base)
    loads[2].wait()
    pack(down_f[...].T.astype(BF16), down_all, my_base)

    pl.semaphore_wait(barrier, len(greeted) + ny - 1)

    def chunks():
        e0 = e_tiles // 2
        s0 = s_tiles // 2
        mine = role * (e_rows + s_rows)
        return (
            (True, 0, mine, e0 * TILE),
            (True, 1, mine + e0 * TILE, (e_tiles - e0) * TILE),
            (False, 2, e_rows, s0 * TILE),
            (False, 3, e_rows + s0 * TILE, (s_tiles - s0) * TILE),
        )

    CH = chunks()
    other_row = (1 - role) * (e_rows + s_rows)

    def crosses(step, d, idx):
        return step < half_ring or (step == half_ring and idx % 2 == d)

    def origin(step, d):
        return (z + nz - step) % nz if d == 0 else (z + step) % nz

    def z_copy(a, step, d, ch):
        at = gathers[a].at[pl.ds(pl.multiple_of(origin(step - 1, d) * size + ch[2], TILE), ch[3]), :]
        return pltpu.make_async_remote_copy(
            at, at, zsend.at[a, d, step - 1, ch[1]], zrecv.at[a, d, step - 1, ch[1]],
            device_id={"fs": z_r if d == 0 else z_l}, device_id_type=MESH,
        )

    def z_arrival(a, step, d, ch):
        at = gathers[a].at[pl.ds(pl.multiple_of(origin(step, d) * size + ch[2], TILE), ch[3]), :]
        return pltpu.make_async_remote_copy(
            at, at, zsend.at[a, d, step - 1, ch[1]], zrecv.at[a, d, step - 1, ch[1]],
            device_id={"fs": z_r if d == 0 else z_l}, device_id_type=MESH,
        )

    def x_copy(a, step, d, ch, row):
        at = gathers[a].at[pl.ds(pl.multiple_of(origin(step, d) * size + row, TILE), ch[3]), :]
        return pltpu.make_async_remote_copy(
            at, at, xsend.at[a, d, step - 1, ch[1]], xrecv.at[a, d, step - 1, ch[1]],
            device_id={"grp": g_x}, device_id_type=MESH,
        )

    sent = []

    def send_own(a):
        for ch in CH:
            for d in range(2):
                copy = z_copy(a, 1, d, ch)
                copy.start()
                sent.append(copy)

    def receive(a, step):
        for ch in CH:
            for d in range(2):
                if not crosses(step, d, ch[1]):
                    continue
                z_arrival(a, step, d, ch).wait_recv()
                if crosses(step + 1, d, ch[1]):
                    copy = z_copy(a, step + 1, d, ch)
                    copy.start()
                    sent.append(copy)
                if ch[0]:
                    copy = x_copy(a, step, d, ch, ch[2])
                    copy.start()
                    sent.append(copy)

    def wait_x(a, step):
        first = 0
        for ch in CH:
            if not ch[0]:
                continue
            for d in range(2):
                if crosses(step, d, ch[1]):
                    x_copy(a, step, d, ch, other_row + first).wait_recv()
            first += ch[3]

    def slots(step):
        if step == 0:
            return 0, 1
        return 2 * step - 1, (2 if step < half_ring else 1)

    def block_of(step, i):
        return (z + (2 * i - 1) * step + nz) % nz

    def up_compute(step):
        _, count = slots(step)

        @pl.loop(0, count)
        def _(i):
            b = block_of(step, i)
            w = unpack(up_all, pl.multiple_of(b * size, TILE), cols, rows)
            part = lax.dot_general(normed[b], w, (((1,), (1,)), ((), ())), preferred_element_type=F32)
            if step == 0:
                acts[...] = part
            else:
                acts[...] += part

    def down_compute(step):
        first, count = slots(step)

        @pl.loop(0, count)
        def _(i):
            b = block_of(step, i)
            w = unpack(down_all, pl.multiple_of(b * size, TILE), cols, rows)
            part = jnp.dot(hid[...], w, preferred_element_type=F32)
            own[first + i] = part[: n_tok // 2]
            pair_out[first + i] = part[n_tok // 2 :].astype(BF16)

    groups = [(0, 3)] + [(2 * s - 1, 2) for s in range(2, half_ring)] + [(nz - 1, 1)]

    def pair_copy(k):
        first, count = groups[k]
        at = pl.ds(first, count)
        return pltpu.make_async_remote_copy(
            pair_out.at[at], pair_in.at[at], psend.at[k], precv.at[k],
            device_id={"tp": t_core}, device_id_type=MESH,
        )

    def y_copy(gi, k):
        first, count = groups[gi]
        return pltpu.make_async_remote_copy(
            msg_out.at[k - 1, pl.ds(first, count)], msg_in.at[ny - 1 - k, pl.ds(first, count)],
            ysend.at[gi, k - 1], yrecv.at[gi, ny - 1 - k], device_id=peer(k), device_id_type=MESH,
        )

    def send_pair(k):
        copy = pair_copy(k)
        copy.start()
        sent.append(copy)

    def send_y(gi):
        first, count = groups[gi]
        pair_copy(gi).wait_recv()

        @pl.loop(0, count)
        def _(i):
            j = first + i
            total = own[j] + pair_in[j].astype(F32)
            keep[j] = total[:q]
            rounded = total.astype(BF16)
            for k in range(1, ny):
                msg_out[k - 1, j] = rounded[k * q : (k + 1) * q]

        @pl.loop(1, ny)
        def _(k):
            y_copy(gi, k).start()

    def sum_y(gi):
        first, count = groups[gi]

        @pl.loop(1, ny)
        def _(k):
            y_copy(gi, k).wait_recv()

        @pl.loop(0, count)
        def _(i):
            j = first + i
            total = keep[j]
            for k in range(ny - 1):
                total += msg_in[k, j].astype(F32)
            step = (j + 1) // 2
            b = (z + (1 - 2 * (j % 2)) * step + nz) % nz
            mixed[b] = total

    send_own(0)

    loads[3].wait()

    @pl.loop(0, n_tok // TILE)
    def _(r):
        at = pl.ds(pl.multiple_of(r * TILE, TILE), TILE)
        values = tok[at, :].astype(F32)
        mean = jnp.mean(values * values, axis=1, keepdims=True)
        scaled = (values * lax.rsqrt(mean + 1e-06)).astype(BF16)
        for b in range(nz):
            normed[b, at, :] = scaled[:, b * rows : (b + 1) * rows]

    up_compute(0)

    for step in range(1, half_ring + 1):
        receive(0, step)
        if step == half_ring - 1:
            send_own(1)
        if step >= 3:
            wait_x(0, step - 2)
            up_compute(step - 2)

    for step in range(1, half_ring + 1):
        receive(1, step)
        if step <= 2:
            wait_x(0, half_ring - 2 + step)
            up_compute(half_ring - 2 + step)
        if step == 2:
            active = jnp.maximum(acts[...], 0.0)
            hidden = (active * active).astype(BF16)
            to = lax.broadcasted_iota(jnp.int32, (n_tok, n_tok), 0)
            src = lax.broadcasted_iota(jnp.int32, (n_tok, n_tok), 1)
            half_bits = (n_tok // 2).bit_length() - 1
            q_bits = q.bit_length() - 1
            half = lax.shift_right_logical(to, half_bits)
            hop = lax.shift_right_logical(to & (n_tok // 2 - 1), q_bits)
            want = ((hop + y) & (ny - 1)) * (CORES * q) + (half ^ c) * q + (to & (q - 1))
            order = (src == want).astype(F32).astype(BF16)
            hid[...] = jnp.dot(order, hidden, preferred_element_type=F32).astype(BF16)
            down_compute(0)
        if step >= 3:
            wait_x(1, step - 2)
            down_compute(step - 2)
            if step >= 4:
                send_pair(step - 4)
            if step >= 5:
                send_y(step - 5)

    n_groups = len(groups)
    send_pair(half_ring - 3)
    send_y(half_ring - 4)
    wait_x(1, half_ring - 1)
    down_compute(half_ring - 1)
    send_pair(n_groups - 2)
    send_y(n_groups - 3)
    wait_x(1, half_ring)
    down_compute(half_ring)
    send_pair(n_groups - 1)
    send_y(n_groups - 2)
    send_y(n_groups - 1)
    for gi in range(n_groups):
        sum_y(gi)

    for copy in sent:
        copy.wait_send()

    @pl.loop(1, ny)
    def _(k):
        for gi in range(n_groups):
            y_copy(gi, k).wait_send()


def final_kernel(rows, cols, per, up_all, down_all, mixed, up_ready, down_ready, mixed_out):
    size = pack_rows(cols, rows)
    first = pl.program_id(0) * per
    for i in range(per):
        base = pl.multiple_of((first + i) * size, TILE)
        at = pl.ds(i * rows, rows)
        up_ready[:, at] = unpack(up_all, base, cols, rows)
        down_ready[:, at] = unpack(down_all, base, cols, rows)

    @pl.when(pl.program_id(0) == 0)
    def _():
        for b in range(mixed.shape[0]):
            mixed_out[:, b * rows : (b + 1) * rows] = mixed[b].astype(BF16)


def per_device(nz, ntp, tokens, norm_gain, up_master, down_master):
    rows, cols = up_master.shape
    n_tok, d = tokens.shape
    ny = ntp // CORES
    q = n_tok // ntp
    size = pack_rows(cols, rows)
    half_ring = nz // 2
    n_groups = half_ring
    dma = pltpu.SemaphoreType.DMA
    in_vmem = pl.BlockSpec(memory_space=pltpu.VMEM)
    half = n_tok // 2
    up_all, down_all, mixed = pl.pallas_call(
        functools.partial(main_kernel, nz, ntp, rows, cols),
        out_shape=(
            pltpu.VMEM((nz * size, LANES), BF16),
            pltpu.VMEM((nz * size, LANES), BF16),
            pltpu.VMEM((nz, q, rows), F32),
        ),
        in_specs=[pl.BlockSpec(memory_space=pltpu.HBM)] * 4,
        out_specs=(in_vmem, in_vmem, in_vmem),
        scratch_shapes=[
            pltpu.VMEM((n_tok, d), BF16),
            pltpu.VMEM((1, rows), F32),
            pltpu.VMEM((rows, cols), F32),
            pltpu.VMEM((rows, cols), F32),
            pltpu.VMEM((nz, n_tok, rows), BF16),
            pltpu.VMEM((n_tok, cols), F32),
            pltpu.VMEM((n_tok, cols), BF16),
            pltpu.VMEM((nz, half, rows), F32),
            pltpu.VMEM((nz, half, rows), BF16),
            pltpu.VMEM((nz, half, rows), BF16),
            pltpu.VMEM((ny - 1, nz, q, rows), BF16),
            pltpu.VMEM((ny - 1, nz, q, rows), BF16),
            pltpu.VMEM((nz, q, rows), F32),
            dma((4,)),
            dma((2, 2, half_ring, 4)),
            dma((2, 2, half_ring, 4)),
            dma((2, 2, half_ring, 2)),
            dma((2, 2, half_ring, 2)),
            dma((n_groups,)),
            dma((n_groups,)),
            dma((n_groups, ny - 1)),
            dma((n_groups, ny - 1)),
        ],
        compiler_params=pltpu.CompilerParams(
            collective_id=0, has_side_effects=True, vmem_limit_bytes=40 * 1024 * 1024
        ),
        name="gather_and_mix",
    )(*(pltpu.with_memory_space_constraint(v, pltpu.HBM) for v in (tokens, norm_gain.reshape(1, rows), up_master, down_master)))
    per = GROUPS
    up_ready, down_ready, mixed_out = pl.pallas_call(
        functools.partial(final_kernel, rows, cols, per),
        grid=(nz // per,),
        out_shape=(
            pltpu.HBM((cols, d), BF16),
            pltpu.HBM((cols, d), BF16),
            pltpu.HBM((q, d), BF16),
        ),
        in_specs=[in_vmem] * 3,
        out_specs=(
            pl.BlockSpec((cols, per * rows), lambda i: (0, i)),
            pl.BlockSpec((cols, per * rows), lambda i: (0, i)),
            pl.BlockSpec((q, d), lambda i: (0, 0)),
        ),
        compiler_params=pltpu.CompilerParams(vmem_limit_bytes=20 * 1024 * 1024),
        name="write_out",
    )(up_all, down_all, mixed)
    return up_ready.T, down_ready.T, mixed_out


def solution(mesh):
    return jax.shard_map(
        functools.partial(per_device, mesh.shape["fs"], mesh.shape["tp"]),
        mesh=mesh,
        in_specs=(P(("grp", "fs"), None), P("fs"), P("fs", "tp"), P("fs", "tp")),
        out_specs=(P("grp", "tp"), P("grp", "tp"), P(("grp", "fs", "tp"), None)),
        check_vma=False,
    )
```

time: 259 us -> 177 us (0.68)
  waiting for transfers between devices: 199 us -> 0 us
  Pallas kernels: 0 us -> 176 us
  local copies, waits for them, and re-layouts: 20.8 us -> 0 us
  between operations: 14.1 us -> 0.64 us
  starting transfers between devices: 13.1 us -> 0 us
  other arithmetic: 5.49 us -> 0 us
  matrix products: 5.45 us -> 0 us
    pallas_call x0 -> x2, Pallas kernels: none -> 176 us  [the longest x1 171 us: per_device(): pl.pallas_call(functools.partial(main_kernel, nz, ntp, rows, cols), out_s...]
    all_gather x1 -> x0, waiting for transfers between devices: 169 us -> none  [sent_together(): result = lax.all_gather(both, axis, axis=dim, tiled=True)]
    all_to_all x1 -> x0, waiting for transfers between devices: 30.2 us -> none  [summed_on_arrival(): parts = lax.all_to_all(cut_along(array, dim, size), axis, 0, 0, tiled=True)]
    all_to_all x1 -> x0, starting transfers between devices: 13 us -> none  [summed_on_arrival(): parts = lax.all_to_all(cut_along(array, dim, size), axis, 0, 0, tiled=True)]
    unnamed x2 -> x0, local copies, waits for them, and re-layouts: 11.3 us -> none
    split x1 -> x0, local copies, waits for them, and re-layouts: 8.35 us -> none  [sent_together(): jnp.split(result, [sum(widths[:k]) for k in range(1, len(widths))], axis=...]
    dot_general x1 -> x0, matrix products: 5.45 us -> none  [per_device(): lax.dot_general(hidden, down_ready, (((1,), (1,)), ((), ())), preferred_e...]
  transfers between devices with their start and end apart: 2 -> 0, of which waited for: 2 -> 0; matrix products, arithmetic and copies ran while one was open for 8% -> 0% of each run, Pallas kernels for 0% -> 0%
where the time goes in v1:
time: 177 us
  Pallas kernels  176 us (99%)
    pallas_call x1, Pallas kernels, per_device(): pl.pallas_call(functools.partial(main_kernel, nz, ntp, rows, cols), out_s...  171 us
    pallas_call x1, Pallas kernels, per_device(): pl.pallas_call(functools.partial(final_kernel, rows, cols, per), grid=(nz...  4.9 us

profile of v1, /device:TPU:5, one launch (start us, length us, event | category | flops | bytes accessed | tf_op | source)
XLA Modules:
  0.0 176.8 jit_solution(16578318670361772177)
XLA Ops:
  0.6 171.3 %gather_and_mix.1 = (bf16[12544,128]{1,0:T(8,128)(2,1)S(1)}, bf16[12544,128]{1,0:T(8,128)(2,1)S(1)}, f32[16,4,224]{2,1,0:T(4,128)S(1)}) custom-call(bf16[128,3584]{1,0:T(8,128)(2,1)} %tokens.1, f32[1,224]{1,0:T(1,128)} %bitcast.3, f32[224,448]{1,0:T(8,128)} %up_master.1, f32[224,448]{1,0:T(8,128)} %down_master.1), custom_call_target="tpu_custom_call" | custom-call | tf_op jit(solution)/shard_map/gather_and_mix/pallas_call | solution.py:363
  171.9 4.9 %write_out.1 = (bf16[448,3584]{1,0:T(8,128)(2,1)}, bf16[448,3584]{1,0:T(8,128)(2,1)}, bf16[4,3584]{1,0:T(4,128)(2,1)}) custom-call(bf16[12544,128]{1,0:T(8,128)(2,1)S(1)} %get-tuple-element.9.up_all, bf16[12544,128]{1,0:T(8,128)(2,1)S(1)} %get-tuple-element.10.down_all, f32[16,4,224]{2,1,0:T(4,128)S(1)} %get-tuple-element.11.mixed), custom_call_target="tpu_custom_call" | custom-call | tf_op jit(solution)/shard_map/write_out/pallas_call | solution.py:402

commit v2 on v0

v2 whole, which is shorter than its diff:
```python
import functools

import jax
import jax.numpy as jnp
from jax import lax
from jax.experimental import pallas as pl
from jax.experimental.pallas import tpu as pltpu
from jax.sharding import PartitionSpec as P

MESH = pl.DeviceIdType.MESH
LANES = 128
TILE = 16
GROUPS = 4
CORES = 2
BF16, F32 = jnp.bfloat16, jnp.float32


def pack_rows(rows, cols):
    whole = cols // LANES * LANES
    return rows * (whole // LANES) + rows * (cols - whole) // LANES


def pack(value, ref, base):
    rows, cols = value.shape
    whole = cols // LANES
    for k in range(whole):
        ref[pl.ds(base + k * rows, rows), :] = value[:, k * LANES : (k + 1) * LANES]
    if cols % LANES:
        part = rows // GROUPS
        rest = value[:, whole * LANES :]
        side = jnp.concatenate([rest[k * part : (k + 1) * part] for k in range(GROUPS)], axis=1)
        for k in range(side.shape[1] // LANES):
            ref[pl.ds(base + whole * rows + k * part, part), :] = side[:, k * LANES : (k + 1) * LANES]


def unpack(ref, base, rows, cols):
    whole = cols // LANES
    parts = [ref[pl.ds(base + k * rows, rows), :] for k in range(whole)]
    width = cols - whole * LANES
    if width:
        part = rows // GROUPS
        side = jnp.concatenate(
            [ref[pl.ds(base + whole * rows + k * part, part), :] for k in range(GROUPS * width // LANES)], axis=1
        )
        parts.append(jnp.concatenate([side[:, k * width : (k + 1) * width] for k in range(GROUPS)], axis=0))
    return jnp.concatenate(parts, axis=1)


def main_kernel(
    nz, ntp, rows, cols,
    tokens, gain, up_master, down_master,
    up_out, down_out, mixed,
    tok, gain_v, up_f, down_f, up_all, down_all, normed, acts, hid, own, pair_out, pair_in, msg_out, msg_in, keep,
    load_sem, zsend, zrecv, xsend, xrecv, psend, precv, ysend, yrecv, right_in, x_in, core_in, y_in,
):
    g, z, t = lax.axis_index("grp"), lax.axis_index("fs"), lax.axis_index("tp")
    y, c = t // CORES, t % CORES
    ny = ntp // CORES
    role = g % 2
    cut = nz - nz // 3
    last, late = nz - 1, nz - cut
    near = z == 0
    z_r, z_l = {"fs": (z + 1) % nz}, {"fs": (z + nz - 1) % nz}
    g_x = {"grp": g + 1 - 2 * role}
    t_core = {"tp": t + 1 - 2 * c}
    size = pack_rows(cols, rows)
    tiles = size // TILE
    e_half = tiles // 5 + (tiles % 5 > 2)
    e_rows = 2 * e_half * TILE
    s_rows = size - 2 * e_rows
    q = mixed.shape[0]
    n_tok = tok.shape[0]
    half_tok = n_tok // 2
    wide = GROUPS * rows
    gathers = (up_all, down_all)

    loads = [
        pltpu.make_async_copy(src, dst, load_sem.at[k])
        for k, (src, dst) in enumerate(((up_master, up_f), (gain, gain_v), (down_master, down_f), (tokens, tok)))
    ]
    for copy in loads:
        copy.start()

    def peer(k):
        return {"tp": ((y + k) % ny) * CORES + c}

    def signal(sem, who):
        pl.semaphore_signal(sem, inc=1, device_id=who, device_id_type=MESH)

    barrier = pltpu.get_barrier_semaphore()

    @pl.when(z < last)
    def _():
        signal(barrier, z_r)

    @pl.when(z == 0)
    def _():
        signal(barrier, z_l)

    @pl.loop(jnp.where(z > 0, y + 1, 0), jnp.where(z > 0, ny, y))
    def _(k):
        signal(barrier, {"tp": k * CORES + c})

    @pl.when(c == 1)
    def _():
        signal(barrier, t_core)

    @pl.when(role == 1)
    def _():
        signal(barrier, g_x)

    my_base = pl.multiple_of(z * size, TILE)
    loads[0].wait()
    loads[1].wait()
    pack((gain_v[...] * up_f[...].T).astype(BF16), up_all, my_base)

    neighbours = (z > 0).astype(jnp.int32) + (z == last).astype(jnp.int32)
    y_first = jnp.where(z > 0, y, ny - 1 - y)
    greetings = neighbours + y_first + (1 - c) + (1 - role)

    @pl.when(greetings > 0)
    def _():
        pl.semaphore_wait(barrier, greetings)


    @pl.when(z > 0)
    def _():
        signal(right_in, z_l)

    @pl.loop(jnp.where(z > 0, 0, y + 1), jnp.where(z > 0, y, ny))
    def _(k):
        signal(y_in, {"tp": k * CORES + c})

    @pl.when(c == 0)
    def _():
        signal(core_in, t_core)

    @pl.when(role == 0)
    def _():
        signal(x_in, g_x)

    mine, theirs = role * (e_rows + s_rows), (1 - role) * (e_rows + s_rows)
    step = e_half * TILE
    kinds = ((0, mine, step), (1, mine + step, step), (2, e_rows, s_rows))

    def part(a, b, row, count):
        return gathers[a].at[pl.ds(pl.multiple_of(b * size + row, TILE), count), :]

    def z_copy(d, a, b, kind):
        i, row, count = kind
        at = part(a, b, row, count)
        return pltpu.make_async_remote_copy(
            at, at, zsend.at[d, a, b, i], zrecv.at[a, b, i], device_id=z_r if d == 0 else z_l, device_id_type=MESH
        )

    def x_copy(a, b, i, row):
        at = part(a, b, row + i * step, step)
        return pltpu.make_async_remote_copy(
            at, at, xsend.at[a, b, i], xrecv.at[a, b, i], device_id=g_x, device_id_type=MESH
        )

    def goes_right(b):
        straight = (z >= b) & ((z < last) | (b >= cut))
        return straight | ((z < b) & (b >= cut) & (z < cut - 1))

    def goes_left(b):
        return jnp.where(b < cut, z >= 1, z >= cut + 1)

    def own_sends(d, a):
        for kind in kinds:
            z_copy(d, a, z, kind).start()

    def receive(a, b, d, onward):
        for kind in kinds:
            z_copy(d, a, b, kind).wait_recv()

            @pl.when(onward)
            def _():
                z_copy(d, a, b, kind).start()

            if kind[0] < 2:
                x_copy(a, b, kind[0], mine).start()

    def wait_x(a, b):
        @pl.when(b != z)
        def _():
            for i in range(2):
                x_copy(a, b, i, theirs).wait_recv()

    def add_up(b):
        wait_x(0, b)
        w = unpack(up_all, pl.multiple_of(b * size, TILE), cols, rows)
        acts[...] += lax.dot_general(normed[b], w, (((1,), (1,)), ((), ())), preferred_element_type=F32)

    @pl.when(goes_left(z))
    def _():
        own_sends(1, 0)

    @pl.when(z == last)
    def _():
        own_sends(0, 0)

    loads[2].wait()
    pack(down_f[...].T.astype(BF16), down_all, my_base)

    loads[3].wait()

    @pl.loop(0, n_tok // TILE)
    def _(r):
        at = pl.ds(pl.multiple_of(r * TILE, TILE), TILE)
        values = tok[at, :].astype(F32)
        mean = jnp.mean(values * values, axis=1, keepdims=True)
        scaled = (values * lax.rsqrt(mean + 1e-06)).astype(BF16)
        for b in range(nz):
            normed[b, at, :] = scaled[:, b * rows : (b + 1) * rows]

    @pl.when(goes_left(z))
    def _():
        own_sends(1, 1)

    @pl.when(z < last)
    def _():
        pl.semaphore_wait(right_in, 1)
        own_sends(0, 0)

    @pl.when(z < cut)
    def _():
        own_sends(0, 1)

    acts[...] = jnp.zeros_like(acts)
    add_up(z)

    @pl.when(role == 1)
    def _():
        pl.semaphore_wait(x_in, 1)

    def from_left(a, s):
        b = (z + nz - 1 - s) % nz
        receive(a, b, 0, goes_right(b))

    before = jnp.where(z < cut, 0, z - cut)

    @pl.loop(0, before)
    def _(s):
        from_left(0, s)

    @pl.when(z >= cut)
    def _():
        own_sends(0, 1)

    @pl.loop(0, before)
    def _(s):
        from_left(1, s)

    above = jnp.where(z < cut, cut - 1 - z, last - z)
    lag = GROUPS

    @pl.loop(0, above)
    def _(s):
        turn = s - (above - 2)

        @pl.when(near & (turn >= 0))
        def _():
            @pl.loop(turn, jnp.minimum(2 * turn + 1, late))
            def _(i):
                from_left(0, i)

        for a in range(2):
            receive(a, z + 1 + s, 1, goes_left(z + 1 + s))

        @pl.when((z < cut) & (s >= lag) & (s - lag < z))
        def _():
            for a in range(2):
                from_left(a, s - lag)

        @pl.when(s >= lag)
        def _():
            add_up(z + 1 + s - lag)

    @pl.loop(jnp.where(z < cut, jnp.minimum(z, jnp.maximum(above - lag, 0)), before), z)
    def _(s):
        for a in range(2):
            from_left(a, s)

    @pl.when(z < cut)
    def _():
        @pl.loop(jnp.where(near, min(3, late), 0), late)
        def _(s):
            from_left(0, z + s)

    done = jnp.maximum(above - lag, 0)

    @pl.loop(done, last)
    def _(s):
        b = jnp.where(s < above, z + 1 + s, s - above)
        add_up(jnp.where((z < cut) & (s >= cut - 1), last - (s - (cut - 1)), b))

    active = jnp.maximum(acts[...], 0.0)
    hidden = (active * active).astype(BF16)
    to = lax.broadcasted_iota(jnp.int32, (n_tok, n_tok), 0)
    src = lax.broadcasted_iota(jnp.int32, (n_tok, n_tok), 1)
    half_bits = half_tok.bit_length() - 1
    q_bits = q.bit_length() - 1
    half = lax.shift_right_logical(to, half_bits)
    hop = lax.shift_right_logical(to & (half_tok - 1), q_bits)
    want = ((hop + y) & (ny - 1)) * (CORES * q) + (half ^ c) * q + (to & (q - 1))
    order = (src == want).astype(F32).astype(BF16)
    hid[...] = jnp.dot(order, hidden, preferred_element_type=F32).astype(BF16)

    n_groups = nz // GROUPS

    def columns(k):
        return pl.ds(k * wide, wide)

    def join(source, out, k):
        for i in range(GROUPS):
            base = (k * GROUPS + i) * size
            out[:, k * wide + i * rows : k * wide + (i + 1) * rows] = unpack(source, base, cols, rows)

    def pair_copy(k):
        return pltpu.make_async_remote_copy(
            pair_out.at[k], pair_in.at[k], psend.at[k], precv.at[k], device_id=t_core, device_id_type=MESH
        )

    def y_copy(k, hops):
        return pltpu.make_async_remote_copy(
            msg_out.at[k, hops - 1], msg_in.at[k, ny - 1 - hops],
            ysend.at[k, hops - 1], yrecv.at[k, ny - 1 - hops], device_id=peer(hops), device_id_type=MESH,
        )

    def mix(k):
        for i in range(GROUPS):
            wait_x(1, k * GROUPS + i)
        join(down_all, down_out, k)
        total = jnp.dot(hid[...], down_out[:, columns(k)], preferred_element_type=F32)
        pair_out[k] = total[half_tok:].astype(BF16)
        own[k] = total[:half_tok]

    def send_y(k):
        pair_copy(k).wait_recv()
        total = own[k] + pair_in[k].astype(F32)
        keep[k] = total[:q]
        rounded = total.astype(BF16)
        for hops in range(1, ny):
            msg_out[k, hops - 1] = rounded[hops * q : (hops + 1) * q]

        @pl.loop(1, ny)
        def _(hops):
            y_copy(k, hops).start()

    def sum_y(k):
        @pl.loop(1, ny)
        def _(hops):
            y_copy(k, hops).wait_recv()

        total = keep[k]
        for i in range(ny - 1):
            total += msg_in[k, i].astype(F32)
        mixed[:, columns(k)] = total.astype(BF16)

    @pl.when(c == 1)
    def _():
        pl.semaphore_wait(core_in, 1)

    early = cut // GROUPS
    turns = list(range(early)) + list(reversed(range(early, n_groups)))
    for i, k in enumerate(turns):
        if i == early:
            send_y(turns[i - 1])

            @pl.when(z < cut)
            def _():
                @pl.loop(0, late)
                def _(s):
                    from_left(1, z + s)

        mix(k)
        pair_copy(k).start()
        if i == 0:
            others = jnp.where(z > 0, ny - 1 - y, y)

            @pl.when(others > 0)
            def _():
                pl.semaphore_wait(y_in, others)
        elif i != early:
            send_y(turns[i - 1])
    join(up_all, up_out, 0)
    send_y(turns[-1])
    for k in range(1, n_groups):
        join(up_all, up_out, k)

    @pl.loop(0, nz)
    def _(b):
        for a in range(2):
            @pl.when(b != z)
            def _():
                for i in range(2):
                    x_copy(a, b, i, mine).wait_send()

            @pl.when(goes_right(b))
            def _():
                for kind in kinds:
                    z_copy(0, a, b, kind).wait_send()

            by_left = (b >= z) & ((b < cut) | (z >= cut))

            @pl.when(by_left & goes_left(b))
            def _():
                for kind in kinds:
                    z_copy(1, a, b, kind).wait_send()

    for i, k in enumerate(turns):
        pair_copy(k).wait_send()
        if i == n_groups - 1:
            for before_k in turns[:-1]:
                @pl.loop(1, ny)
                def _(hops):
                    y_copy(before_k, hops).wait_send()
        sum_y(k)

    @pl.loop(1, ny)
    def _(hops):
        y_copy(turns[-1], hops).wait_send()


def final_kernel(up_v, down_v, mixed_v, up_ready, down_ready, mixed_out, sem):
    copies = []
    rows = up_v.shape[0] // GROUPS
    for a, (src, dst) in enumerate(((up_v, up_ready), (down_v, down_ready))):
        for k in range(GROUPS):
            at = pl.ds(k * rows, rows)
            copies.append(pltpu.make_async_copy(src.at[at], dst.at[at], sem.at[a * GROUPS + k]))
    copies.append(pltpu.make_async_copy(mixed_v, mixed_out, sem.at[2 * GROUPS]))
    for copy in copies:
        copy.start()
    for copy in copies:
        copy.wait()


def per_device(nz, ntp, tokens, norm_gain, up_master, down_master):
    rows, cols = up_master.shape
    n_tok, d = tokens.shape
    ny = ntp // CORES
    q = n_tok // ntp
    size = pack_rows(cols, rows)
    n_groups, wide = nz // GROUPS, GROUPS * rows
    dma, regular = pltpu.SemaphoreType.DMA, pltpu.SemaphoreType.REGULAR
    in_vmem, in_hbm = pl.BlockSpec(memory_space=pltpu.VMEM), pl.BlockSpec(memory_space=pltpu.HBM)
    half = n_tok // 2
    results = pl.pallas_call(
        functools.partial(main_kernel, nz, ntp, rows, cols),
        out_shape=(pltpu.VMEM((cols, d), BF16), pltpu.VMEM((cols, d), BF16), pltpu.VMEM((q, d), BF16)),
        in_specs=[in_hbm] * 4,
        out_specs=(in_vmem, in_vmem, in_vmem),
        scratch_shapes=[
            pltpu.VMEM((n_tok, d), BF16),
            pltpu.VMEM((1, rows), F32),
            pltpu.VMEM((rows, cols), F32),
            pltpu.VMEM((rows, cols), F32),
            pltpu.VMEM((nz * size, LANES), BF16),
            pltpu.VMEM((nz * size, LANES), BF16),
            pltpu.VMEM((nz, n_tok, rows), BF16),
            pltpu.VMEM((n_tok, cols), F32),
            pltpu.VMEM((n_tok, cols), BF16),
            pltpu.VMEM((n_groups, half, wide), F32),
            pltpu.VMEM((n_groups, half, wide), BF16),
            pltpu.VMEM((n_groups, half, wide), BF16),
            pltpu.VMEM((n_groups, ny - 1, q, wide), BF16),
            pltpu.VMEM((n_groups, ny - 1, q, wide), BF16),
            pltpu.VMEM((n_groups, q, wide), F32),
            dma((4,)),
            dma((2, 2, nz, 3)),
            dma((2, nz, 3)),
            dma((2, nz, 2)),
            dma((2, nz, 2)),
            dma((n_groups,)),
            dma((n_groups,)),
            dma((n_groups, ny - 1)),
            dma((n_groups, ny - 1)),
            regular,
            regular,
            regular,
            regular,
        ],
        compiler_params=pltpu.CompilerParams(
            collective_id=0, has_side_effects=True, vmem_limit_bytes=40 * 1024 * 1024
        ),
        name="gather_and_mix",
    )(*(pltpu.with_memory_space_constraint(v, pltpu.HBM) for v in (tokens, norm_gain.reshape(1, rows), up_master, down_master)))
    up_ready, down_ready, mixed_out = pl.pallas_call(
        final_kernel,
        out_shape=(pltpu.HBM((cols, d), BF16), pltpu.HBM((cols, d), BF16), pltpu.HBM((q, d), BF16)),
        in_specs=[in_vmem] * 3,
        out_specs=(in_hbm, in_hbm, in_hbm),
        scratch_shapes=[dma((2 * GROUPS + 1,))],
        compiler_params=pltpu.CompilerParams(vmem_limit_bytes=4 * 1024 * 1024),
        name="write_out",
    )(*results)
    return up_ready.T, down_ready.T, mixed_out


def solution(mesh):
    return jax.shard_map(
        functools.partial(per_device, mesh.shape["fs"], mesh.shape["tp"]),
        mesh=mesh,
        in_specs=(P(("grp", "fs"), None), P("fs"), P("fs", "tp"), P("fs", "tp")),
        out_specs=(P("grp", "tp"), P("grp", "tp"), P(("grp", "fs", "tp"), None)),
        check_vma=False,
    )
```

time: 259 us -> 151 us (0.58)
  waiting for transfers between devices: 199 us -> 0 us
  Pallas kernels: 0 us -> 150 us
  local copies, waits for them, and re-layouts: 20.8 us -> 0 us
  between operations: 14.1 us -> 0.64 us
  starting transfers between devices: 13.1 us -> 0 us
  other arithmetic: 5.49 us -> 0 us
  matrix products: 5.45 us -> 0 us
    all_gather x1 -> x0, waiting for transfers between devices: 169 us -> none  [sent_together(): result = lax.all_gather(both, axis, axis=dim, tiled=True)]
    pallas_call x0 -> x2, Pallas kernels: none -> 150 us  [the longest x1 147 us: per_device(): pl.pallas_call(functools.partial(main_kernel, nz, ntp, rows, cols), out_s...]
    all_to_all x1 -> x0, waiting for transfers between devices: 30.2 us -> none  [summed_on_arrival(): parts = lax.all_to_all(cut_along(array, dim, size), axis, 0, 0, tiled=True)]
    all_to_all x1 -> x0, starting transfers between devices: 13 us -> none  [summed_on_arrival(): parts = lax.all_to_all(cut_along(array, dim, size), axis, 0, 0, tiled=True)]
    unnamed x2 -> x0, local copies, waits for them, and re-layouts: 11.3 us -> none
    split x1 -> x0, local copies, waits for them, and re-layouts: 8.35 us -> none  [sent_together(): jnp.split(result, [sum(widths[:k]) for k in range(1, len(widths))], axis=...]
    dot_general x1 -> x0, matrix products: 5.45 us -> none  [per_device(): lax.dot_general(hidden, down_ready, (((1,), (1,)), ((), ())), preferred_e...]
  transfers between devices with their start and end apart: 2 -> 0, of which waited for: 2 -> 0; matrix products, arithmetic and copies ran while one was open for 8% -> 0% of each run, Pallas kernels for 0% -> 0%
where the time goes in v2:
time: 151 us
  Pallas kernels  150 us (99%)
    pallas_call x1, Pallas kernels, per_device(): pl.pallas_call(functools.partial(main_kernel, nz, ntp, rows, cols), out_s...  147 us

profile of v2, /device:TPU:5, one launch (start us, length us, event | category | flops | bytes accessed | tf_op | source)
XLA Modules:
  0.0 150.7 jit_solution(12694683386999752577)
XLA Ops:
  0.6 147.3 %gather_and_mix.1 = (bf16[448,3584]{1,0:T(8,128)(2,1)S(1)}, bf16[448,3584]{1,0:T(8,128)(2,1)S(1)}, bf16[4,3584]{1,0:T(4,128)(2,1)S(1)}) custom-call(bf16[128,3584]{1,0:T(8,128)(2,1)} %tokens.1, f32[1,224]{1,0:T(1,128)} %bitcast.3, f32[224,448]{1,0:T(8,128)} %up_master.1, f32[224,448]{1,0:T(8,128)} %down_master.1), custom_call_target="tpu_custom_call" | custom-call | tf_op jit(solution)/shard_map/gather_and_mix/pallas_call | solution.py:450
  148.0 2.8 %write_out.1 = (bf16[448,3584]{1,0:T(8,128)(2,1)}, bf16[448,3584]{1,0:T(8,128)(2,1)}, bf16[4,3584]{1,0:T(4,128)(2,1)}) custom-call(bf16[448,3584]{1,0:T(8,128)(2,1)S(1)} %get-tuple-element.9.up_v, bf16[448,3584]{1,0:T(8,128)(2,1)S(1)} %get-tuple-element.10.down_v, bf16[4,3584]{1,0:T(4,128)(2,1)S(1)} %get-tuple-element.11.mixed_v), custom_call_target="tpu_custom_call" | custom-call | tf_op jit(solution)/shard_map/write_out/pallas_call | solution.py:490

commit v3 on v2

--- a/solution.py
+++ b/solution.py
@@ -51,14 +51,14 @@
     tokens, gain, up_master, down_master,
     up_out, down_out, mixed,
     tok, gain_v, up_f, down_f, up_all, down_all, normed, acts, hid, own, pair_out, pair_in, msg_out, msg_in, keep,
-    load_sem, zsend, zrecv, xsend, xrecv, psend, precv, ysend, yrecv, right_in, x_in, core_in, y_in,
+    load_sem, zsend, zsend_own, zrecv, xsend, xrecv, psend, precv, ysend, yrecv, right_in, x_in, core_in, y_in,
 ):
     g, z, t = lax.axis_index("grp"), lax.axis_index("fs"), lax.axis_index("tp")
     y, c = t // CORES, t % CORES
     ny = ntp // CORES
     role = g % 2
-    cut = nz - nz // 3
-    last, late = nz - 1, nz - cut
+    cuts = (nz - nz // 3, nz - nz // 4)
+    last, late = nz - 1, nz // 3
     near = z == 0
     z_r, z_l = {"fs": (z + 1) % nz}, {"fs": (z + nz - 1) % nz}
     g_x = {"grp": g + 1 - 2 * role}
@@ -146,29 +146,33 @@
     def part(a, b, row, count):
         return gathers[a].at[pl.ds(pl.multiple_of(b * size + row, TILE), count), :]
 
-    def z_copy(d, a, b, kind):
+    def z_copy(d, a, b, kind, own_left=False):
         i, row, count = kind
         at = part(a, b, row, count)
+        sem = zsend_own.at[a] if own_left else zsend.at[a, b]
         return pltpu.make_async_remote_copy(
-            at, at, zsend.at[d, a, b, i], zrecv.at[a, b, i], device_id=z_r if d == 0 else z_l, device_id_type=MESH
+            at, at, sem, zrecv.at[a, b, i], device_id=z_r if d == 0 else z_l, device_id_type=MESH
         )
 
-    def x_copy(a, b, i, row):
-        at = part(a, b, row + i * step, step)
+    whole_block = (0, 0, e_rows + s_rows)
+
+    def x_copy(a, b, row, count):
+        at = part(a, b, row, count)
         return pltpu.make_async_remote_copy(
-            at, at, xsend.at[a, b, i], xrecv.at[a, b, i], device_id=g_x, device_id_type=MESH
+            at, at, xsend, xrecv.at[a, b], device_id=g_x, device_id_type=MESH
         )
 
-    def goes_right(b):
+    def goes_right(a, b):
+        cut = cuts[a]
         straight = (z >= b) & ((z < last) | (b >= cut))
         return straight | ((z < b) & (b >= cut) & (z < cut - 1))
 
-    def goes_left(b):
-        return jnp.where(b < cut, z >= 1, z >= cut + 1)
+    def goes_left(a, b):
+        return jnp.where(b < cuts[a], z >= 1, z >= cuts[a] + 1)
 
     def own_sends(d, a):
         for kind in kinds:
-            z_copy(d, a, z, kind).start()
+            z_copy(d, a, z, kind, own_left=d == 1).start()
 
     def receive(a, b, d, onward):
         for kind in kinds:
@@ -179,20 +183,19 @@
                 z_copy(d, a, b, kind).start()
 
             if kind[0] < 2:
-                x_copy(a, b, kind[0], mine).start()
+                x_copy(a, b, kind[1], kind[2]).start()
 
     def wait_x(a, b):
         @pl.when(b != z)
         def _():
-            for i in range(2):
-                x_copy(a, b, i, theirs).wait_recv()
+            x_copy(a, b, theirs, e_rows).wait_recv()
 
     def add_up(b):
         wait_x(0, b)
         w = unpack(up_all, pl.multiple_of(b * size, TILE), cols, rows)
         acts[...] += lax.dot_general(normed[b], w, (((1,), (1,)), ((), ())), preferred_element_type=F32)
 
-    @pl.when(goes_left(z))
+    @pl.when(goes_left(0, z))
     def _():
         own_sends(1, 0)
 
@@ -214,7 +217,7 @@
         for b in range(nz):
             normed[b, at, :] = scaled[:, b * rows : (b + 1) * rows]
 
-    @pl.when(goes_left(z))
+    @pl.when(goes_left(1, z))
     def _():
         own_sends(1, 1)
 
@@ -223,7 +226,7 @@
         pl.semaphore_wait(right_in, 1)
         own_sends(0, 0)
 
-    @pl.when(z < cut)
+    @pl.when(z < cuts[0])
     def _():
         own_sends(0, 1)
 
@@ -236,64 +239,74 @@
 
     def from_left(a, s):
         b = (z + nz - 1 - s) % nz
-        receive(a, b, 0, goes_right(b))
-
-    before = jnp.where(z < cut, 0, z - cut)
-
-    @pl.loop(0, before)
+        receive(a, b, 0, goes_right(a, b))
+
+    before = [jnp.where(z < cut, 0, z - cut) for cut in cuts]
+
+    @pl.loop(0, before[0])
     def _(s):
         from_left(0, s)
 
-    @pl.when(z >= cut)
+    @pl.when(z >= cuts[0])
     def _():
         own_sends(0, 1)
 
-    @pl.loop(0, before)
+    @pl.loop(0, before[1])
     def _(s):
         from_left(1, s)
 
-    above = jnp.where(z < cut, cut - 1 - z, last - z)
+    above = [jnp.where(z < cut, cut - 1 - z, last - z) for cut in cuts]
+    longest = jnp.maximum(above[0], above[1])
     lag = GROUPS
-
-    @pl.loop(0, above)
+    taken = jnp.where(z < cuts[0], jnp.minimum(z, jnp.maximum(longest - lag, 0)), before[1])
+
+    @pl.loop(0, longest)
     def _(s):
-        turn = s - (above - 2)
+        turn = s - (above[0] - 2)
 
         @pl.when(near & (turn >= 0))
         def _():
-            @pl.loop(turn, jnp.minimum(2 * turn + 1, late))
+            first = turn * (turn + 1) // 2
+
+            @pl.loop(jnp.minimum(first, late), jnp.minimum(first + turn + 1, late))
             def _(i):
                 from_left(0, i)
 
         for a in range(2):
-            receive(a, z + 1 + s, 1, goes_left(z + 1 + s))
-
-        @pl.when((z < cut) & (s >= lag) & (s - lag < z))
+            @pl.when(s < above[a])
+            def _():
+                receive(a, z + 1 + s, 1, goes_left(a, z + 1 + s))
+
+        @pl.when((z < cuts[0]) & (s >= lag) & (s - lag < z))
         def _():
             for a in range(2):
                 from_left(a, s - lag)
 
-        @pl.when(s >= lag)
+        @pl.when((s >= lag) & (s - lag < above[0]))
         def _():
             add_up(z + 1 + s - lag)
 
-    @pl.loop(jnp.where(z < cut, jnp.minimum(z, jnp.maximum(above - lag, 0)), before), z)
+    @pl.loop(taken, z)
     def _(s):
         for a in range(2):
-            from_left(a, s)
-
-    @pl.when(z < cut)
-    def _():
-        @pl.loop(jnp.where(near, min(3, late), 0), late)
+            @pl.when(s >= (before[0] if a == 0 else 0))
+            def _():
+                from_left(a, s)
+
+    turns_near = max(cuts) - 1 - (cuts[0] - 3)
+
+    @pl.when(z < cuts[0])
+    def _():
+        @pl.loop(jnp.where(near, min(turns_near * (turns_near + 1) // 2, late), 0), late)
         def _(s):
             from_left(0, z + s)
 
-    done = jnp.maximum(above - lag, 0)
+    done = jnp.minimum(jnp.maximum(longest - lag, 0), above[0])
 
     @pl.loop(done, last)
     def _(s):
-        b = jnp.where(s < above, z + 1 + s, s - above)
-        add_up(jnp.where((z < cut) & (s >= cut - 1), last - (s - (cut - 1)), b))
+        b = jnp.where(s < above[0], z + 1 + s, s - above[0])
+        add_up(jnp.where((z < cuts[0]) & (s >= cuts[0] - 1), last - (s - (cuts[0] - 1)), b))
 
     active = jnp.maximum(acts[...], 0.0)
     hidden = (active * active).astype(BF16)
@@ -325,7 +338,12 @@
     def y_copy(k, hops):
         return pltpu.make_async_remote_copy(
             msg_out.at[k, hops - 1], msg_in.at[k, ny - 1 - hops],
-            ysend.at[k, hops - 1], yrecv.at[k, ny - 1 - hops], device_id=peer(hops), device_id_type=MESH,
+            ysend.at[k], yrecv.at[k], device_id=peer(hops), device_id_type=MESH,
+        )
+
+    def y_all(k):
+        return pltpu.make_async_remote_copy(
+            msg_out.at[k], msg_in.at[k], ysend.at[k], yrecv.at[k], device_id=peer(1), device_id_type=MESH
         )
 
     def mix(k):
@@ -349,10 +367,7 @@
             y_copy(k, hops).start()
 
     def sum_y(k):
-        @pl.loop(1, ny)
-        def _(hops):
-            y_copy(k, hops).wait_recv()
-
+        y_all(k).wait_recv()
         total = keep[k]
         for i in range(ny - 1):
             total += msg_in[k, i].astype(F32)
@@ -362,18 +377,22 @@
     def _():
         pl.semaphore_wait(core_in, 1)
 
-    early = cut // GROUPS
+    late_down = nz - cuts[1]
+
+    def late_from_left(first, end):
+        @pl.when(z < cuts[1])
+        def _():
+            @pl.loop(first, end)
+            def _(s):
+                from_left(1, z + s)
+
+    early = cuts[1] // GROUPS
     turns = list(range(early)) + list(reversed(range(early, n_groups)))
+    late_from_left(0, 1)
     for i, k in enumerate(turns):
         if i == early:
             send_y(turns[i - 1])
-
-            @pl.when(z < cut)
-            def _():
-                @pl.loop(0, late)
-                def _(s):
-                    from_left(1, z + s)
-
+            late_from_left(min(early, late_down), late_down)
         mix(k)
         pair_copy(k).start()
         if i == 0:
@@ -384,43 +403,37 @@
                 pl.semaphore_wait(y_in, others)
         elif i != early:
             send_y(turns[i - 1])
+        if 0 < i < min(early, late_down):
+            late_from_left(i, i + 1)
     join(up_all, up_out, 0)
     send_y(turns[-1])
     for k in range(1, n_groups):
         join(up_all, up_out, k)
 
+    at = up_all.at[pl.ds(0, (nz - 1) * 2 * e_rows), :]
+    pltpu.make_async_remote_copy(at, at, xsend, xrecv.at[0, 0], device_id=g_x, device_id_type=MESH).wait_send()
+
+    for a in range(2):
+        @pl.when(goes_left(a, z))
+        def _():
+            z_copy(1, a, z, whole_block, own_left=True).wait_send()
+
     @pl.loop(0, nz)
     def _(b):
         for a in range(2):
-            @pl.when(b != z)
+            by_left = (b > z) & ((b < cuts[a]) | (z >= cuts[a]))
+
+            @pl.when(goes_right(a, b) | (by_left & goes_left(a, b)))
             def _():
-                for i in range(2):
-                    x_copy(a, b, i, mine).wait_send()
-
-            @pl.when(goes_right(b))
-            def _():
-                for kind in kinds:
-                    z_copy(0, a, b, kind).wait_send()
-
-            by_left = (b >= z) & ((b < cut) | (z >= cut))
-
-            @pl.when(by_left & goes_left(b))
-            def _():
-                for kind in kinds:
-                    z_copy(1, a, b, kind).wait_send()
+                z_copy(0, a, b, whole_block).wait_send()
 
     for i, k in enumerate(turns):
         pair_copy(k).wait_send()
         if i == n_groups - 1:
             for before_k in turns[:-1]:
-                @pl.loop(1, ny)
-                def _(hops):
-                    y_copy(before_k, hops).wait_send()
+                y_all(before_k).wait_send()
         sum_y(k)
-
-    @pl.loop(1, ny)
-    def _(hops):
-        y_copy(turns[-1], hops).wait_send()
+    y_all(turns[-1]).wait_send()
 
 
 def final_kernel(up_v, down_v, mixed_v, up_ready, down_ready, mixed_out, sem):
@@ -469,14 +482,15 @@
             pltpu.VMEM((n_groups, ny - 1, q, wide), BF16),
             pltpu.VMEM((n_groups, q, wide), F32),
             dma((4,)),
-            dma((2, 2, nz, 3)),
+            dma((2, nz)),
+            dma((2,)),
             dma((2, nz, 3)),
-            dma((2, nz, 2)),
-            dma((2, nz, 2)),
+            dma,
+            dma((2, nz)),
             dma((n_groups,)),
             dma((n_groups,)),
-            dma((n_groups, ny - 1)),
-            dma((n_groups, ny - 1)),
+            dma((n_groups,)),
+            dma((n_groups,)),
             regular,
             regular,
             regular,

time: 151 us -> 147 us (0.974)
  Pallas kernels: 150 us -> 146 us
    pallas_call x1, Pallas kernels: 147 us -> 143 us  [per_device(): pl.pallas_call(functools.partial(main_kernel, nz, ntp, rows, cols), out_s...]
where the time goes in v3:
time: 147 us
  Pallas kernels  146 us (99%)
    pallas_call x1, Pallas kernels, per_device(): pl.pallas_call(functools.partial(main_kernel, nz, ntp, rows, cols), out_s...  143 us

profile of v3, /device:TPU:5, one launch (start us, length us, event | category | flops | bytes accessed | tf_op | source)
XLA Modules:
  0.0 146.9 jit_solution(13067587404712029613)
XLA Ops:
  0.6 143.5 %gather_and_mix.1 = (bf16[448,3584]{1,0:T(8,128)(2,1)S(1)}, bf16[448,3584]{1,0:T(8,128)(2,1)S(1)}, bf16[4,3584]{1,0:T(4,128)(2,1)S(1)}) custom-call(bf16[128,3584]{1,0:T(8,128)(2,1)} %tokens.1, f32[1,224]{1,0:T(1,128)} %bitcast.3, f32[224,448]{1,0:T(8,128)} %up_master.1, f32[224,448]{1,0:T(8,128)} %down_master.1), custom_call_target="tpu_custom_call" | custom-call | tf_op jit(solution)/shard_map/gather_and_mix/pallas_call | solution.py:463
  144.1 2.8 %write_out.1 = (bf16[448,3584]{1,0:T(8,128)(2,1)}, bf16[448,3584]{1,0:T(8,128)(2,1)}, bf16[4,3584]{1,0:T(4,128)(2,1)}) custom-call(bf16[448,3584]{1,0:T(8,128)(2,1)S(1)} %get-tuple-element.9.up_v, bf16[448,3584]{1,0:T(8,128)(2,1)S(1)} %get-tuple-element.10.down_v, bf16[4,3584]{1,0:T(4,128)(2,1)S(1)} %get-tuple-element.11.mixed_v), custom_call_target="tpu_custom_call" | custom-call | tf_op jit(solution)/shard_map/write_out/pallas_call | solution.py:504
